TPU v7x, 32 devices: a whole 2x2x4 slice. The times are simulated.
32 devices in a mesh: sp: 16 (over z, y, x), tp: 2 (over core).
Axes of the slice: x: 2, y: 2, z: 4, core: 2. Of those that a mesh axis runs over, the one named last changes fastest.
Arguments:
- resid: bfloat16 [3072, 2048], P(('sp', 'tp')), may hold values from -6 to 6
- queries: bfloat16 [3072, 2048], P('sp', 'tp'), may hold values from -8 to 8
- keys: bfloat16 [3072, 512], P('sp', 'tp'), may hold values from -8 to 8
- values: bfloat16 [3072, 512], P('sp', 'tp'), may hold values from -6 to 6
- log_gates: float32 [3072, 32], P('sp', 'tp'), may hold values from -1536 to 0, as said below
- out_gate: bfloat16 [3072, 2048], P('sp', 'tp'), may hold values from -8 to 8
- out_weight: bfloat16 [2048, 2048], P('tp'), may hold values from -0.125 to 0.125
- post_gain: float32 [2048], replicated, may hold values from 0.1 to 1.9
- pre_gain: float32 [2048], replicated, may hold values from 0.1 to 1.9
- ffn_gain: float32 [2048], replicated, may hold values from 0.1 to 1.9
- gate_weight: bfloat16 [2048, 5632], P('sp', 'tp'), may hold values from -0.125 to 0.125
- up_weight: bfloat16 [2048, 5632], P('sp', 'tp'), may hold values from -0.125 to 0.125
- down_weight: bfloat16 [5632, 2048], P('tp', 'sp'), may hold values from -0.078125 to 0.078125
Outputs:
- result: bfloat16 [3072, 2048], P(('sp', 'tp'))
Inputs may be any that keep to these rules, and one draw needn't show every extreme that they name: Each head's column of log_gates never rises from one position to the next, and its first entry is at most 0.
All inputs are finite; a program needn't handle non-finite values.
Results may differ from a plain program's by a relative error of at most 0.017.
Values may be sent and summed in bfloat16 or wider, within the bound.
A program may use at most 128 MiB of HBM per device.

v0:
```python
import jax
import jax.numpy as jnp
from jax import lax
from jax.sharding import PartitionSpec as P

HD = 64


EPS = 1e-06
KEY_BLOCK = 512


def rms_scale(rows, gain):
    mean_sq = jnp.mean(rows * rows, axis=-1, keepdims=True)
    return rows * lax.rsqrt(mean_sq + EPS) * gain


def shards(
    resid,
    queries,
    keys,
    values,
    log_gates,
    out_gate,
    out_weight,
    post_gain,
    pre_gain,
    ffn_gain,
    gate_weight,
    up_weight,
    down_weight,
):
    rows = queries.shape[0]
    head_size = HD
    kv_local = keys.shape[1] // head_size
    q_local = queries.shape[1] // head_size
    group = q_local // kv_local
    scale = head_size ** (-0.5)
    offset = lax.axis_index("sp") * rows
    last = offset + rows - 1
    query_pos = offset + jnp.arange(rows, dtype=jnp.int32)
    key_gates = lax.all_gather(log_gates, "sp", axis=0, tiled=True)
    query_blocks = queries.reshape(rows, kv_local, group, head_size)
    query_gates = log_gates.reshape(rows, kv_local, group).transpose(1, 2, 0)

    def key_block(carry, key_rows, value_rows, start):
        count = key_rows.shape[0]

        def compute(state):
            top, denom, accum = state
            scores = (
                jnp.einsum(
                    "tkgd,skd->kgts",
                    query_blocks,
                    key_rows.reshape(count, kv_local, head_size),
                    preferred_element_type=jnp.float32,
                )
                * scale
            )
            gates_here = (
                lax.dynamic_slice_in_dim(key_gates, start, count, 0)
                .reshape(count, kv_local, group)
                .transpose(1, 2, 0)
            )
            scores = scores + query_gates[:, :, :, None] - gates_here[:, :, None, :]
            causal = (start + jnp.arange(count, dtype=jnp.int32))[None, :] <= query_pos[:, None]
            scores = jnp.where(causal[None, None], scores, -jnp.inf)
            new_top = jnp.maximum(top, jnp.max(scores, axis=-1))
            shrink = jnp.exp(top - new_top)
            weights = jnp.exp(scores - new_top[..., None])
            denom = denom * shrink + jnp.sum(weights, axis=-1)
            accum = accum * shrink[..., None] + jnp.einsum(
                "kgts,skd->kgtd",
                weights.astype(jnp.bfloat16),
                value_rows.reshape(count, kv_local, head_size),
                preferred_element_type=jnp.float32,
            )
            return (new_top, denom, accum)

        def keep(state):
            return state

        return lax.cond(start <= last, compute, keep, carry)

    start_state = (
        jnp.full((kv_local, group, rows), -1e30, jnp.float32),
        jnp.zeros((kv_local, group, rows), jnp.float32),
        jnp.zeros((kv_local, group, rows, head_size), jnp.float32),
    )
    carry = start_state
    key_rows = lax.all_gather(keys, "sp", axis=0, tiled=True)
    value_rows = lax.all_gather(values, "sp", axis=0, tiled=True)
    count = key_rows.shape[0]
    blocks = count // KEY_BLOCK
    key_split = key_rows.reshape(blocks, KEY_BLOCK, key_rows.shape[1])
    value_split = value_rows.reshape(blocks, KEY_BLOCK, value_rows.shape[1])

    def advance(state, item):
        index, key_part, value_part = item
        return (key_block(state, key_part, value_part, index * KEY_BLOCK), None)

    carry, _ = lax.scan(
        advance, carry, (jnp.arange(blocks, dtype=jnp.int32), key_split, value_split)
    )
    top, denom, accum = carry
    attended = (accum / denom[..., None]).transpose(2, 0, 1, 3).reshape(rows, q_local * head_size)
    gated = (attended * jax.nn.sigmoid(out_gate.astype(jnp.float32))).astype(jnp.bfloat16)
    projected = lax.psum_scatter(
        jnp.dot(gated, out_weight, preferred_element_type=jnp.float32).astype(jnp.bfloat16),
        "tp",
        scatter_dimension=0,
        tiled=True,
    ).astype(jnp.float32)
    mixed = resid.astype(jnp.float32) + rms_scale(projected, post_gain)
    normed = rms_scale(mixed, pre_gain).astype(jnp.bfloat16)
    normed_all = lax.all_gather(normed, "tp", axis=0, tiled=True)
    gate = jnp.dot(
        normed_all,
        lax.all_gather(gate_weight, "sp", axis=0, tiled=True),
        preferred_element_type=jnp.float32,
    )
    up = jnp.dot(
        normed_all,
        lax.all_gather(up_weight, "sp", axis=0, tiled=True),
        preferred_element_type=jnp.float32,
    )
    hidden = (jax.nn.silu(gate) * up).astype(jnp.bfloat16)
    ffn_partial = jnp.dot(
        hidden,
        lax.all_gather(down_weight, "sp", axis=1, tiled=True),
        preferred_element_type=jnp.float32,
    )
    ffn = lax.psum_scatter(
        ffn_partial.astype(jnp.bfloat16), "tp", scatter_dimension=0, tiled=True
    ).astype(jnp.float32)
    return (mixed + rms_scale(ffn, ffn_gain)).astype(jnp.bfloat16)


def solution(mesh):
    in_specs = (
        P(("sp", "tp"), None),
        P("sp", "tp"),
        P("sp", "tp"),
        P("sp", "tp"),
        P("sp", "tp"),
        P("sp", "tp"),
        P("tp", None),
        P(),
        P(),
        P(),
        P("sp", "tp"),
        P("sp", "tp"),
        P("tp", "sp"),
    )
    out_specs = P(("sp", "tp"), None)
    return jax.shard_map(shards, mesh=mesh, in_specs=in_specs, out_specs=out_specs, check_vma=False)
```

profile of v0, /device:TPU:0, one launch (start us, length us, event | category | flops | bytes accessed | tf_op | source)
XLA Modules:
  0.0 712.2 jit_solution(13522817512439941888)
XLA Ops:
  6.5 0.0 all-gather.7.cloned.1.call-start
  6.5 0.7 all-gather.7.cloned.1.call-update
  7.3 0.0 all-gather.9.cloned.1.call-start
  7.3 0.7 all-gather.9.cloned.1.call-update
  8.0 0.0 reduce-scatter.3.cloned.1.call-start
  8.1 0.7 reshape.101
  8.8 44.2 %all-gather = f32[16,192,16]{1,2,0:T(8,128)S(1)} all-gather(f32[1,192,16]{1,2,0:T(8,128)} %bitcast.74), channel_id=1, replica_groups=mesh['sp'=16,'tp'=2] {'sp'}, dimensions={0}, use_global_device_ids=true | all-gather | bytes 208896 | tf_op jit(solution)/shard_map/all_gather | solution.py:42
  52.9 0.2 copy.27
  53.1 0.1 reshape.105
  53.2 2.0 copy.26
  55.2 15.7 %all-gather.7.cloned.1.call-done = bf16[3072,256]{1,0:T(8,128)(2,1)} async-done(((bf16[192,256]{1,0:T(8,128)(2,1)}), bf16[3072,256]{1,0:T(8,128)(2,1)}) %all-gather.7.cloned.1.call-update) | async-done | bytes 1572880 | tf_op jit(solution)/shard_map/all_gather | solution.py:91
  70.9 1.7 copy.28
  72.7 57.8 %all-gather.9.cloned.1.call-done = bf16[3072,256]{1,0:T(8,128)(2,1)} async-done(((bf16[192,256]{1,0:T(8,128)(2,1)}), bf16[3072,256]{1,0:T(8,128)(2,1)}) %all-gather.9.cloned.1.call-update) | async-done | bytes 1572880 | tf_op jit(solution)/shard_map/all_gather | solution.py:92
  130.4 1.7 copy.29
  132.2 1.1 broadcast_in_dim.42
  133.3 17.4 %while.15 = (s32[]{:T(128)}, f32[4,4,192]{2,1,0:T(4,128)S(1)}, f32[4,4,192]{2,1,0:T(4,128)S(1)}, f32[4,4,192,64]{2,3,1,0:T(8,128)}, s32[6]{0:T(128)S(1)}, /*inde...) while((s32[]{:T(128)}, f32[4,4,192]{2,1,0:T(4,128)S(1)}, ...), condition=%wide.region_5.6_spmd.clone, body=%wide.region_0.5_spmd.clone.sunk | while | flops 429890240 | bytes 29568428 | solution.py:102
  133.3 0.6 dynamic_slice.31
  134.5 9.6 %conditional.3 = ((f32[4,4,192]{2,1,0:T(4,128)S(1)}, f32[4,4,192]{2,1,0:T(4,128)S(1)}, f32[4,4,192,64]{2,3,1,0:T(8,128)})) conditional(s32[]{:T(128)} %convert_element_type.96, (f32[4,4,192]{2,1,0:T(4,128)S(1)}, f32[4,4,192]{2,1,0:T(4,128)S(1)}, f32[4,4,192,64]{2,3,1,0:T(8,128)}) %tuple.43, (s32[]{:T(128)}, s32[]{:T(128)}, ...), branch_computations={%region_1.1_spmd, %region_2.4_spmd} | conditional | flops 429890240 | bytes 29567370 | solution.py:83
  134.5 0.1 constant_dynamic-slice_fusion.1
  134.7 0.1 broadcast_compare_fusion
  134.8 0.0 copy-start.1
  134.9 3.4 fusion.6
  138.2 2.5 fusion.5
  140.8 0.0 copy-done.1
  140.8 2.3 fusion.10
  143.1 0.0 copy-start.2
  143.1 1.0 copy-done.2
  144.1 0.6 dynamic_slice.31
  145.4 0.6 dynamic_slice.31
  146.7 0.6 dynamic_slice.31
  148.0 0.6 dynamic_slice.31
  149.3 0.6 dynamic_slice.31
  150.6 1.3 broadcast_divide_fusion
  152.0 0.3 copy.30
  152.3 0.0 copy-start.3
  152.3 0.0 copy-start.4
  152.3 0.0 copy-start.5
  152.3 4.3 convolution_convert_fusion.1
  156.6 0.0 reduce-scatter.3.cloned.1.call-update
  156.6 0.0 all-gather.11.cloned.1.call-start
  156.7 0.5 all-gather.11.cloned.1.call-update
  157.2 0.0 all-gather.13.cloned.1.call-start
  157.3 0.5 all-gather.13.cloned.1.call-update
  157.8 0.0 all-gather.15.cloned.1.call-start
  157.8 0.5 all-gather.15.cloned.1.call-update
  158.4 0.0 reduce-scatter.5.cloned.1.call-start
  158.4 53.0 %reduce-scatter.3.cloned.1.call-done = bf16[96,2048]{1,0:T(8,128)(2,1)} async-done(((bf16[192,2048]{1,0:T(8,128)(2,1)}), bf16[96,2048]{1,0:T(8,128)(2,1)}) %reduce-scatter.3.cloned.1.call-update) | async-done | bytes 393232 | tf_op jit(solution)/shard_map/reduce_scatter | solution.py:108
  211.4 1.2 fusion.16
  212.6 0.0 copy-done.3
  212.6 0.0 copy-done.4
  212.6 1.3 multiply_reduce_fusion
  214.0 0.0 copy-done.5
  214.0 1.3 multiply_convert_fusion
  215.3 2.5 all_gather.24
  217.8 138.8 %all-gather.11.cloned.1.call-done = bf16[2048,2816]{1,0:T(8,128)(2,1)} async-done(((bf16[128,2816]{1,0:T(8,128)(2,1)}), bf16[2048,2816]{1,0:T(8,128)(2,1)}) %all-gather.11.cloned.1.call-update) | async-done | bytes 11534352 | tf_op jit(solution)/shard_map/all_gather | solution.py:119
  356.6 8.0 %fusion.26 = f32[192,2816]{1,0:T(8,128)} fusion(bf16[192,2048]{1,0:T(8,128)(2,1)S(1)} %all_gather.24, bf16[2048,2816]{1,0:T(8,128)(2,1)} %all-gather.11.cloned.1.call-done), kind=kOutput, calls=%fused_computation.46 | convolution fusion | flops 2214592512 | bytes 14483456 | tf_op jit(solution)/shard_map/dot_general | solution.py:117
  364.6 134.2 %all-gather.13.cloned.1.call-done = bf16[2048,2816]{1,0:T(8,128)(2,1)} async-done(((bf16[128,2816]{1,0:T(8,128)(2,1)}), bf16[2048,2816]{1,0:T(8,128)(2,1)}) %all-gather.13.cloned.1.call-update) | async-done | bytes 11534352 | tf_op jit(solution)/shard_map/all_gather | solution.py:124
  498.8 182.8 %all-gather.15.cloned.1.call-done = bf16[2816,2048]{1,0:T(8,128)(2,1)} async-done(((bf16[2816,128]{1,0:T(8,128)(2,1)}), bf16[2816,2048]{1,0:T(8,128)(2,1)}) %all-gather.15.cloned.1.call-update) | async-done | bytes 11534352 | tf_op jit(solution)/shard_map/all_gather | solution.py:130
  681.6 13.9 %convolution_convert_fusion = bf16[192,2048]{1,0:T(8,128)(2,1)} fusion(bf16[2816,2048]{1,0:T(8,128)(2,1)} %all-gather.15.cloned.1.call-done, bf16[192,2048]{1,0:T(8,128)(2,1)S(1)} %all_gather.24, bf16[2048,2816]{1,0:T(8,128)(2,1)} %all-gather.13.cloned.1.call-done, f32[192,2816]{1,0:T(8,128)} %fusion.26), kind=kOutput, calls=%fused_computation.23 | convolution fusion | flops 4432822272 | bytes 26804224 | tf_op jit(solution)/shard_map/dot_general | solution.py:128
  695.5 0.0 reduce-scatter.5.cloned.1.call-update
  695.5 6.5 reduce-scatter.5.cloned.1.call-done
  702.0 1.2 fusion.19
  703.2 0.0 copy-done
  703.2 2.1 fusion.22
  (27 shorter events, 0.2 us)
Async XLA Ops:
  6.5 64.4 %all-gather.7.cloned.1.call-start = ((), (), s32[]{:S(2)}) async-start(), calls=%async_computation.2 | async-start | bytes 1671168 | tf_op jit(solution)/shard_map/all_gather | solution.py:91
  7.3 123.2 %all-gather.9.cloned.1.call-start = ((), (), s32[]{:S(2)}) async-start(), calls=%async_computation.3 | async-start | bytes 1671168 | tf_op jit(solution)/shard_map/all_gather | solution.py:92
  8.0 203.4 %reduce-scatter.3.cloned.1.call-start = ((), (), s32[]{:S(2)}) async-start(), calls=%async_computation.4 | async-start | bytes 1179648 | tf_op jit(solution)/shard_map/reduce_scatter | solution.py:108
  134.8 6.0 copy-start.1
  143.1 1.0 copy-start.2
  152.3 60.3 %copy-start.3 = (bf16[96,2048]{1,0:T(8,128)(2,1)S(1)}, bf16[96,2048]{1,0:T(8,128)(2,1)}, u32[]{:S(2)}) copy-start(bf16[96,2048]{1,0:T(8,128)(2,1)} %param.17) | copy-start | bytes 1179652
  152.3 60.3 %copy-start.4 = (f32[2048]{0:T(1024)S(1)}, f32[2048]{0:T(1024)}, u32[]{:S(2)}) copy-start(f32[2048]{0:T(1024)} %param.24) | copy-start | bytes 24580
  152.3 61.7 %copy-start.5 = (f32[2048]{0:T(1024)S(1)}, f32[2048]{0:T(1024)}, u32[]{:S(2)}) copy-start(f32[2048]{0:T(1024)} %param.25) | copy-start | bytes 24580
  156.6 200.0 %all-gather.11.cloned.1.call-start = ((), (), s32[]{:S(2)}) async-start(), calls=%async_computation.5 | async-start | bytes 12255232 | tf_op jit(solution)/shard_map/all_gather | solution.py:119
  157.2 341.6 %all-gather.13.cloned.1.call-start = ((), (), s32[]{:S(2)}) async-start(), calls=%async_computation.6 | async-start | bytes 12255232 | tf_op jit(solution)/shard_map/all_gather | solution.py:124
  157.8 523.8 %all-gather.15.cloned.1.call-start = ((), (), s32[]{:S(2)}) async-start(), calls=%async_computation.7 | async-start | bytes 12255232 | tf_op jit(solution)/shard_map/all_gather | solution.py:130
  158.4 543.6 %reduce-scatter.5.cloned.1.call-start = ((), (), s32[]{:S(2)}) async-start(), calls=%async_computation.8 | async-start | bytes 1179648 | tf_op jit(solution)/shard_map/reduce_scatter | solution.py:133
  364.6 338.6 %copy-start = (bf16[96,2048]{1,0:T(8,128)(2,1)S(1)}, bf16[96,2048]{1,0:T(8,128)(2,1)}, u32[]{:S(2)}) copy-start(bf16[96,2048]{1,0:T(8,128)(2,1)} %reduce-scatter.3.cloned.1.call-done) | copy-start | bytes 1179652
  364.6 338.6 %copy-start.6 = (f32[2048]{0:T(1024)S(1)}, f32[2048]{0:T(1024)}, u32[]{:S(2)}) copy-start(f32[2048]{0:T(1024)} %param.26) | copy-start | bytes 24580
Sparse Core Ops, SparseCore 0:
  10.1 60.7 all-gather.6
  73.7 56.6 all-gather.8
  156.8 54.6 reduce-scatter.2
  214.0 142.5 all-gather.10
  359.2 139.5 all-gather.12
  501.4 180.2 all-gather.14
  695.6 6.3 reduce-scatter.4
where the time goes:
time: 713 us; the launch traced here: 712 us
  waiting for transfers between devices  592 us (83%)
  blocking collectives  46.7 us (7%)
  matrix products  31.8 us (4%)
  between operations  13.6 us (2%)
  local copies, waits for them, and re-layouts  12.7 us (2%)
  other arithmetic  11.1 us (2%)
    all_gather x1, waiting for transfers between devices, shards(): lax.all_gather(down_weight, 'sp', axis=1, tiled=True)  183 us
    all_gather x1, waiting for transfers between devices, shards(): lax.all_gather(gate_weight, 'sp', axis=0, tiled=True)  139 us
    all_gather x1, waiting for transfers between devices, shards(): lax.all_gather(up_weight, 'sp', axis=0, tiled=True)  134 us
    all_gather x1, waiting for transfers between devices, shards(): value_rows = lax.all_gather(values, 'sp', axis=0, tiled=True)  57.8 us
    reduce_scatter x1, waiting for transfers between devices, shards(): lax.psum_scatter(jnp.dot(gated, out_weight, preferred_element_type=jnp.fl...  53 us
    all_gather x1, blocking collectives, shards(): key_gates = lax.all_gather(log_gates, 'sp', axis=0, tiled=True)  44.2 us
    all_gather x1, waiting for transfers between devices, shards(): key_rows = lax.all_gather(keys, 'sp', axis=0, tiled=True)  15.7 us
  transfers between devices with their start and end apart: 7, of which 7 were waited for; matrix products, arithmetic and copies ran while one was open for 2% of the time, Pallas kernels for 0%

commit v1 on v0

--- a/solution.py
+++ b/solution.py
@@ -1,6 +1,10 @@
+import functools
+
 import jax
 import jax.numpy as jnp
 from jax import lax
+from jax.experimental import pallas as pl
+from jax.experimental.pallas import tpu as pltpu
 from jax.sharding import PartitionSpec as P
 
 HD = 64
@@ -136,7 +140,277 @@
     return (mixed + rms_scale(ffn, ffn_gain)).astype(jnp.bfloat16)
 
 
+MESH = pl.DeviceIdType.MESH
+ANY = pl.BlockSpec(memory_space=pl.ANY)
+
+
+def to(peer):
+    return {"sp": peer}
+
+
+def greet(peers):
+    barrier = pltpu.get_barrier_semaphore()
+    for peer in peers:
+        pl.semaphore_signal(barrier, inc=1, device_id=peer, device_id_type=MESH)
+    pl.semaphore_wait(barrier, len(peers))
+
+
+def remote(src, dst, send, recv, peer):
+    return pltpu.make_async_remote_copy(
+        src_ref=src, dst_ref=dst, send_sem=send, recv_sem=recv, device_id=peer, device_id_type=MESH
+    )
+
+
+def swap_kernel(n, groups, x_ref, o_ref, send, recv, local):
+    me = lax.axis_index("sp")
+    size = n // groups
+    slot = lax.rem(me, size)
+    base = me - slot
+    peers = [base + lax.rem(slot + j, size) for j in range(1, size)]
+    greet([to(p) for p in peers])
+    copies = []
+    for j, p in enumerate(peers):
+        c = remote(x_ref.at[p - base], o_ref.at[slot], send.at[j], recv.at[j], to(p))
+        c.start()
+        copies.append(c)
+    own = pltpu.make_async_copy(x_ref.at[slot], o_ref.at[slot], local)
+    own.start()
+    own.wait()
+    for c in copies:
+        c.wait()
+
+
+def swap(x, n, groups, cid):
+    size = n // groups
+    return pl.pallas_call(
+        functools.partial(swap_kernel, n, groups),
+        out_shape=jax.ShapeDtypeStruct(x.shape, x.dtype),
+        in_specs=[ANY],
+        out_specs=ANY,
+        scratch_shapes=[
+            pltpu.SemaphoreType.DMA((size - 1,)),
+            pltpu.SemaphoreType.DMA((size - 1,)),
+            pltpu.SemaphoreType.DMA,
+        ],
+        compiler_params=pltpu.CompilerParams(collective_id=cid, has_side_effects=True),
+    )(x)
+
+
+def partner_kernel(x_ref, o_ref, send, recv):
+    other = 1 - lax.axis_index("tp")
+    peer = {"tp": other}
+    greet([peer])
+    c = remote(x_ref.at[other], o_ref, send, recv, peer)
+    c.start()
+    c.wait()
+
+
+def partner(x, cid):
+    return pl.pallas_call(
+        partner_kernel,
+        out_shape=jax.ShapeDtypeStruct(x.shape[1:], x.dtype),
+        in_specs=[ANY],
+        out_specs=ANY,
+        scratch_shapes=[pltpu.SemaphoreType.DMA, pltpu.SemaphoreType.DMA],
+        compiler_params=pltpu.CompilerParams(collective_id=cid, has_side_effects=True),
+    )(x)
+
+
+def spread_kernel(n, groups, rows_ref, g_ref, u_ref, d_ref, all_ref, go_ref, uo_ref, do_ref,
+                  wsend, wrecv, wlocal, asend, arecv, psend, precv, alocal):
+    me = lax.axis_index("sp")
+    core = lax.axis_index("tp")
+    size = n // groups
+    slot = lax.rem(me, size)
+    base = me - slot
+    mate = {"tp": 1 - core}
+    order = [lax.rem(me + j, n) for j in range(1, n)]
+    greet([mate] + [to(p) for p in order])
+    pushes = []
+    for j in range(1, size):
+        c = remote(rows_ref, all_ref.at[core, slot], asend.at[j - 1], arecv.at[j - 1],
+                   to(base + lax.rem(slot + j, size)))
+        c.start()
+        pushes.append(c)
+    relays = [remote(rows_ref, all_ref.at[core, slot], psend.at[0], precv.at[0], mate)]
+    relays[0].start()
+    own = pltpu.make_async_copy(rows_ref, all_ref.at[core, slot], alocal)
+    own.start()
+    weights = []
+    parts = ((g_ref, go_ref), (u_ref, uo_ref), (d_ref, do_ref))
+    for j, p in enumerate(order):
+        for k, (src, dst) in enumerate(parts):
+            c = remote(src.at[lax.rem(p, size)], dst.at[me], wsend.at[k, j], wrecv.at[k, j], to(p))
+            c.start()
+            weights.append(c)
+    locals_ = [pltpu.make_async_copy(src.at[slot], dst.at[me], wlocal.at[k])
+               for k, (src, dst) in enumerate(parts)]
+    for c in locals_:
+        c.start()
+    for j in range(1, size):
+        pushes[j - 1].wait()
+        origin = lax.rem(slot + size - j, size)
+        c = remote(all_ref.at[core, origin], all_ref.at[core, origin], psend.at[j], precv.at[j], mate)
+        c.start()
+        relays.append(c)
+    own.wait()
+    for c in relays + locals_ + weights:
+        c.wait()
+
+
+def spread(rows, g, u, d, n, groups, cid):
+    size = n // groups
+    full = lambda w: jax.ShapeDtypeStruct((n,) + w.shape[1:], w.dtype)
+    dma = pltpu.SemaphoreType.DMA
+    return pl.pallas_call(
+        functools.partial(spread_kernel, n, groups),
+        out_shape=(jax.ShapeDtypeStruct((2, size) + rows.shape, rows.dtype), full(g), full(u), full(d)),
+        in_specs=[ANY] * 4,
+        out_specs=(ANY,) * 4,
+        scratch_shapes=[
+            dma((3, n - 1)), dma((3, n - 1)), dma((3,)),
+            dma((size - 1,)), dma((size - 1,)), dma((size,)), dma((size,)), dma,
+        ],
+        compiler_params=pltpu.CompilerParams(collective_id=cid, has_side_effects=True),
+    )(rows, g, u, d)
+
+
+def attend_kernel(block, head, scale, q_ref, k_ref, v_ref, gc_ref, gr_ref, o_ref):
+    index = pl.program_id(0)
+    q = q_ref[...] * jnp.asarray(scale, q_ref.dtype)
+    gc = gc_ref[...]
+
+    def step(kb, carry, diagonal=False):
+        top, acc = carry
+        ks = pl.ds(pl.multiple_of(kb * block, block), block)
+        s = lax.dot_general(q, k_ref[ks, :], (((1,), (1,)), ((), ())), preferred_element_type=jnp.float32)
+        s = s + gc - gr_ref[:, ks]
+        if diagonal:
+            r = lax.broadcasted_iota(jnp.int32, s.shape, 0)
+            c = lax.broadcasted_iota(jnp.int32, s.shape, 1)
+            s = jnp.where(c <= r, s, -1e30)
+        new = jnp.maximum(top, jnp.max(s, axis=1, keepdims=True))
+        p = jnp.exp(s - new).astype(jnp.bfloat16)
+        acc = acc * jnp.exp(top - new) + jnp.dot(p, v_ref[ks, :], preferred_element_type=jnp.float32)
+        return new, acc
+
+    start = (jnp.full((block, 1), -1e30, jnp.float32), jnp.zeros((block, v_ref.shape[1]), jnp.float32))
+    carry = step(index, start, True)
+    _, acc = lax.fori_loop(0, index, step, carry)
+    o_ref[...] = (acc[:, :head] / acc[:, head:head + 1]).astype(o_ref.dtype)
+
+
+def attend(q, k, v, gates, block):
+    total, head = q.shape
+    whole = lambda a: pl.BlockSpec(a.shape, lambda i: (0, 0))
+    row = gates.reshape(1, total)
+    return pl.pallas_call(
+        functools.partial(attend_kernel, block, head, head ** -0.5),
+        grid=(total // block,),
+        out_shape=jax.ShapeDtypeStruct((total, head), jnp.bfloat16),
+        in_specs=[
+            pl.BlockSpec((block, head), lambda i: (i, 0)), whole(k), whole(v),
+            pl.BlockSpec((block, 1), lambda i: (i, 0)), whole(row),
+        ],
+        out_specs=pl.BlockSpec((block, head), lambda i: (i, 0)),
+        compiler_params=pltpu.CompilerParams(
+            dimension_semantics=("arbitrary",), vmem_limit_bytes=40 * 1024 * 1024
+        ),
+    )(q, k, v, gates.reshape(total, 1), row)
+
+
+def halves(x, lanes):
+    *lead, r, h = x.shape
+    f = lanes // h
+    x = x.reshape(*lead, f, r // f, h)
+    return jnp.swapaxes(x, -3, -2).reshape(*lead, r // f, lanes)
+
+
+def unhalves(x, h):
+    *lead, r, lanes = x.shape
+    f = lanes // h
+    x = x.reshape(*lead, r, f, h)
+    return jnp.swapaxes(x, -3, -2).reshape(*lead, r * f, h)
+
+
+LANES = 128
+
+
+def pack(queries, keys, values, log_gates, heads):
+    rows = queries.shape[0]
+    kv = keys.shape[1] // HD
+    group = heads // kv
+    by_head = lambda a, m: jnp.repeat(a.reshape(rows, m, HD).transpose(1, 0, 2), heads // m, axis=0)
+    qk = jnp.concatenate([by_head(queries, heads), by_head(keys, kv)], axis=-1)
+    v = jnp.repeat(halves(values.reshape(rows, kv, HD).transpose(1, 0, 2), LANES), group, axis=0)
+    g = log_gates.T
+    hi = lax.reduce_precision(g, 8, 7)
+    mid = lax.reduce_precision(g - hi, 8, 7)
+    low = g - hi - mid
+    g3 = jnp.stack([hi, mid, low], axis=1).reshape(heads, 3 * rows)
+    pad = -(3 * rows) % (16 * LANES)
+    g3 = jnp.pad(g3, ((0, 0), (0, pad))).reshape(heads, -1, LANES).astype(jnp.bfloat16)
+    return jnp.concatenate([qk, v, g3], axis=1)
+
+
+def unpack(got, rows):
+    n = got.shape[0]
+    qk = got[:, :rows].reshape(n * rows, 2 * HD)
+    v = unhalves(got[:, rows:rows + rows * HD // LANES], HD).reshape(n * rows, HD)
+    g3 = got[:, rows + rows * HD // LANES:].reshape(n, -1)[:, :3 * rows].reshape(n, 3, rows)
+    g3 = g3.astype(jnp.float32)
+    gates = (g3[:, 0] + g3[:, 1]) + g3[:, 2]
+    v = jnp.concatenate([v, jnp.ones_like(v)], axis=1)
+    return qk[:, :HD], qk[:, HD:], v, gates.reshape(n * rows)
+
+
+def fast_shards(n, resid, queries, keys, values, log_gates, out_gate, out_weight, post_gain,
+                pre_gain, ffn_gain, gate_weight, up_weight, down_weight):
+    rows = queries.shape[0]
+    heads = queries.shape[1] // HD
+    width = resid.shape[1]
+    groups = 2
+    size = n // groups
+    ff = gate_weight.shape[1] // size
+    got = swap(pack(queries, keys, values, log_gates, heads), n, 1, 1)
+    q, k, v, gates = unpack(got, rows)
+    att = attend(q, k, v, gates, n * rows // 6)
+    back = swap(halves(att.reshape(n, rows, HD), LANES), n, 1, 2)
+    attended = unhalves(back, HD).transpose(1, 0, 2).reshape(rows, heads * HD).astype(jnp.float32)
+    gated = (attended * jax.nn.sigmoid(out_gate.astype(jnp.float32))).astype(jnp.bfloat16)
+    partial = jnp.dot(gated, out_weight, preferred_element_type=jnp.float32)
+    core = lax.axis_index("tp")
+    partial = partial.astype(jnp.bfloat16).reshape(2, rows // 2, width)
+    mine = lambda a: lax.dynamic_index_in_dim(a, core, 0, keepdims=False).astype(jnp.float32)
+    projected = mine(partial) + partner(partial, 3).astype(jnp.float32)
+    mixed = resid.astype(jnp.float32) + rms_scale(projected, post_gain)
+    normed = rms_scale(mixed, pre_gain).astype(jnp.bfloat16)
+    cut = lambda w: w.reshape(w.shape[0], size, ff).transpose(1, 0, 2)
+    normed_all, gw, uw, dw = spread(
+        normed, cut(gate_weight), cut(up_weight), down_weight.reshape(size, ff, -1), n, groups, 4
+    )
+    x = normed_all.reshape(2 * size * normed.shape[0], width)
+    gate = jnp.dot(x, gw.reshape(width, ff), preferred_element_type=jnp.float32)
+    up = jnp.dot(x, uw.reshape(width, ff), preferred_element_type=jnp.float32)
+    hidden = (jax.nn.silu(gate) * up).astype(jnp.bfloat16)
+    down = dw.transpose(1, 0, 2).reshape(ff, width)
+    part = jnp.dot(hidden, down, preferred_element_type=jnp.float32).astype(jnp.bfloat16)
+    part = part.reshape(2, size * normed.shape[0], width)
+    both = mine(part) + partner(part, 5).astype(jnp.float32)
+    both = both.astype(jnp.bfloat16).reshape(size, normed.shape[0], width)
+    ffn = jnp.sum(swap(both, n, groups, 6).astype(jnp.float32), axis=0)
+    return (mixed + rms_scale(ffn, ffn_gain)).astype(jnp.bfloat16)
+
+
 def solution(mesh):
+    n, cores = mesh.shape["sp"], mesh.shape["tp"]
+
+    def body(*args):
+        queries, gate_weight = args[1], args[10]
+        fits = cores == 2 and queries.shape[1] == n * HD and n % 2 == 0
+        fits = fits and gate_weight.shape[1] % (n * 8) == 0
+        return fast_shards(n, *args) if fits else shards(*args)
+
     in_specs = (
         P(("sp", "tp"), None),
         P("sp", "tp"),
@@ -153,4 +427,4 @@
         P("tp", "sp"),
     )
     out_specs = P(("sp", "tp"), None)
-    return jax.shard_map(shards, mesh=mesh, in_specs=in_specs, out_specs=out_specs, check_vma=False)
+    return jax.shard_map(body, mesh=mesh, in_specs=in_specs, out_specs=out_specs, check_vma=False)

time: 713 us -> 333 us (0.47)
  waiting for transfers between devices: 592 us -> 0 us
  Pallas kernels: 0 us -> 267 us
  blocking collectives: 46.7 us -> 0 us
  between operations: 13.6 us -> 0.41 us
  matrix products: 31.8 us -> 23.1 us
    all_gather x5 -> x0, waiting for transfers between devices: 529 us -> none  [the longest x1 183 us: shards(): lax.all_gather(down_weight, 'sp', axis=1, tiled=True)]
    pallas_call x0 -> x7, Pallas kernels: none -> 267 us  [the longest x1 146 us: spread(): pl.pallas_call(functools.partial(spread_kernel, n, groups), out_shape=(ja...]
    reduce_scatter x2 -> x0, waiting for transfers between devices: 59.5 us -> none  [the longest x1 53 us: shards(): lax.psum_scatter(jnp.dot(gated, out_weight, preferred_element_type=jnp.fl...]
    all_gather x2 -> x0, blocking collectives: 46.7 us -> none  [the longest x1 44.2 us: shards(): key_gates = lax.all_gather(log_gates, 'sp', axis=0, tiled=True)]
    dot_general x5 -> x3, matrix products: 31.8 us -> 23.1 us  [the longest x1 11.9 us: fast_shards(): jnp.dot(hidden, down, preferred_element_type=jnp.float32)]
  transfers between devices with their start and end apart: 7 -> 0, of which waited for: 7 -> 0; matrix products, arithmetic and copies ran while one was open for 2% -> 0% of each run, Pallas kernels for 0% -> 0%
where the time goes in v1:
time: 333 us; the launch traced here: 327 us
  Pallas kernels  267 us (80%)
  matrix products  23.1 us (7%)
  local copies, waits for them, and re-layouts  19.8 us (6%)
  other arithmetic  16.4 us (5%)
    pallas_call x1, Pallas kernels, spread(): pl.pallas_call(functools.partial(spread_kernel, n, groups), out_shape=(ja...  146 us
    pallas_call x3, Pallas kernels, swap(): pl.pallas_call(functools.partial(swap_kernel, n, groups), out_shape=jax.S...  97.8 us
    pallas_call x1, Pallas kernels, attend(): pl.pallas_call(functools.partial(attend_kernel, block, head, head ** (-0....  15 us
    dot_general x1, matrix products, fast_shards(): jnp.dot(hidden, down, preferred_element_type=jnp.float32)  11.9 us
    pallas_call x2, Pallas kernels, partner(): pl.pallas_call(partner_kernel, out_shape=jax.ShapeDtypeStruct(x.shape[1:]...  8.1 us
    unnamed x35, local copies, waits for them, and re-layouts  7.68 us
    dot_general x1, matrix products, fast_shards(): gate = jnp.dot(x, gw.reshape(width, ff), preferred_element_type=jnp.float32)  7.14 us

profile of v1, /device:TPU:0, one launch (start us, length us, event | category | flops | bytes accessed | tf_op | source)
XLA Modules:
  0.0 326.6 jit_solution(6965138849361624880)
XLA Ops:
  0.0 0.8 fusion.8
  0.8 0.1 reshape.177
  0.9 0.0 copy-start.8
  1.0 1.0 copy.20
  2.0 0.2 copy.21
  2.2 1.0 copy.22
  3.2 0.1 reshape.174
  3.3 0.1 copy.24
  3.4 0.1 broadcast_in_dim.5
  3.5 0.0 copy-done.7
  3.5 0.2 copy.18
  3.7 0.4 copy.19
  4.1 0.0 copy-done.8
  4.1 1.0 copy.33
  5.1 0.1 broadcast_in_dim.4
  5.3 1.5 pad_maximum_fusion.x_ref
  6.8 27.6 %shard_map.127 = bf16[16,304,128]{2,1,0:T(8,128)(2,1)} custom-call(bf16[16,304,128]{2,1,0:T(8,128)(2,1)} %pad_maximum_fusion.x_ref), custom_call_target="tpu_custom_call" | custom-call | tf_op jit(solution)/shard_map/pallas_call | solution.py:185
  34.4 0.0 slice-start
  34.4 0.9 slice.31
  35.3 0.1 reshape.193
  35.4 0.1 fusion.6
  35.5 0.1 add.98.gr_ref
  35.6 0.0 slice-done
  35.6 0.3 copy.26
  35.9 0.4 copy.27
  36.2 0.2 concatenate.11.v_ref
  36.4 0.3 copy-done.6
  36.7 0.4 copy.34
  37.0 0.0 slice-start.1
  37.0 1.2 copy.35
  38.2 1.5 copy.36
  39.7 1.2 copy.37
  40.9 0.0 slice-done.1
  40.9 1.4 fusion.11
  42.3 1.4 add.109.gc_ref
  43.7 0.0 copy-start
  43.7 1.1 copy-done
  44.9 1.1 copy-done.1
  46.0 15.0 %shard_map.128 = bf16[3072,64]{1,0:T(8,128)(2,1)S(1)} custom-call(bf16[3072,64]{1,0:T(8,128)(2,1)S(1)} %copy-done.1, bf16[3072,64]{1,0:T(8,128)(2,1)S(1)} %copy-done, bf16[3072,128]{1,0:T(8,128)(2,1)S(1)} %concatenate.11.v_ref, f32[3072,1]{1,0:T(8,128)S(1)} %add.109.gc_ref, f32[1,3072]{1,0:T(1,128)S(1)} %add.98.gr_ref), custom_call_target="tpu_custom_call" | custom-call | tf_op jit(solution)/shard_map/pallas_call | solution.py:307
  61.0 0.3 copy.29
  61.3 1.0 copy.30.x_ref
  62.3 19.1 %shard_map.129 = bf16[16,96,128]{2,1,0:T(8,128)(2,1)} custom-call(bf16[16,96,128]{2,1,0:T(8,128)(2,1)} %copy.30.x_ref), custom_call_target="tpu_custom_call" | custom-call | tf_op jit(solution)/shard_map/pallas_call | solution.py:185
  81.4 1.2 copy.31
  82.6 0.0 copy-start.5
  82.6 0.8 copy.32
  83.5 0.6 reshape.197
  84.1 0.3 fusion.4
  84.4 0.0 copy-start.9
  84.4 4.1 %convolution_convert_fusion.1 = bf16[192,2048]{1,0:T(8,128)(2,1)} fusion(bf16[192,1024]{0,1:T(8,128)(2,1)S(1)} %fusion.4, bf16[1024,2048]{1,0:T(8,128)(2,1)} %param.19), kind=kOutput, calls=%fused_computation.6 | convolution fusion | flops 805699584 | bytes 5373952 | tf_op jit(solution)/shard_map/dot_general | solution.py:381
  88.5 2.1 shard_map.130
  90.6 1.4 multiply_reduce_fusion.2
  92.0 1.4 multiply_reduce_fusion.1
  93.4 1.0 multiply_convert_fusion.rows_ref
  94.5 146.0 %shard_map.131 = (bf16[2,8,96,2048]{3,2,1,0:T(8,128)(2,1)}, bf16[16,128,352]{2,1,0:T(8,128)(2,1)}, bf16[16,128,352]{2,1,0:T(8,128)(2,1)}, bf16[16,352,128]{2,1,0:T(8,128)(2,1)}) custom-call(bf16[96,2048]{1,0:T(8,128)(2,1)} %multiply_convert_fusion.rows_ref, bf16[8,128,352]{2,1,0:T(8,128)(2,1)} %bitcast.111, bf16[8,128,352]{2,1,0:T(8,128)(2,1)} %bitcast.112, ...), custom_call_target="tpu_custom_call" | custom-call | tf_op jit(solution)/shard_map/pallas_call | solution.py:265
  240.5 0.0 copy-start.12
  240.5 7.1 %fusion.12 = f32[1536,352]{0,1:T(8,128)} fusion(bf16[1536,2048]{1,0:T(8,128)(2,1)} %bitcast.128, bf16[2048,352]{1,0:T(8,128)(2,1)} %bitcast.131), kind=kOutput, calls=%fused_computation.39 | convolution fusion | flops 2214592512 | bytes 9895936 | tf_op jit(solution)/shard_map/dot_general | solution.py:393
  247.6 11.9 %convolution_convert_fusion = bf16[1536,2048]{1,0:T(8,128)(2,1)} fusion(bf16[1536,2048]{1,0:T(8,128)(2,1)} %bitcast.129, bf16[2048,352]{1,0:T(8,128)(2,1)S(1)} %bitcast.130, f32[1536,352]{0,1:T(8,128)} %fusion.12, bf16[16,352,128]{2,1,0:T(8,128)(2,1)} %get-tuple-element.12), kind=kOutput, calls=%fused_computation | convolution fusion | flops 4435574784 | bytes 17629184 | tf_op jit(solution)/shard_map/dot_general | solution.py:397
  259.6 6.0 %shard_map.132 = bf16[768,2048]{1,0:T(8,128)(2,1)} custom-call(bf16[2,768,2048]{2,1,0:T(8,128)(2,1)} %bitcast.100), custom_call_target="tpu_custom_call" | custom-call | tf_op jit(solution)/shard_map/pallas_call | solution.py:209
  265.6 6.1 %fusion = bf16[768,2048]{1,0:T(8,128)(2,1)} fusion(bf16[768,2048]{1,0:T(8,128)(2,1)} %shard_map.132, bf16[2,768,2048]{2,1,0:T(8,128)(2,1)} %bitcast.101, s32[]{:T(128)S(6)} %select_n.6), kind=kLoop, calls=%fused_computation.2 | loop fusion | flops 6291456 | bytes 9437188 | tf_op jit(solution)/shard_map/convert_element_type | solution.py:400
  271.7 51.1 %shard_map.133 = bf16[8,96,2048]{2,1,0:T(8,128)(2,1)} custom-call(bf16[8,96,2048]{2,1,0:T(8,128)(2,1)} %bitcast.102), custom_call_target="tpu_custom_call" | custom-call | tf_op jit(solution)/shard_map/pallas_call | solution.py:185
  322.8 0.0 copy-start.11
  322.8 2.5 convert_reduce_fusion
  325.4 0.1 multiply_reduce_fusion
  325.5 1.1 add_convert_fusion
  (25 shorter events, 0.1 us)
Async XLA Ops:
  0.0 3.5 %copy-start.7 = (bf16[192,1024]{1,0:T(8,128)(2,1)S(1)}, bf16[192,1024]{1,0:T(8,128)(2,1)}, u32[]{:S(2)}) copy-start(bf16[192,1024]{1,0:T(8,128)(2,1)} %param.14) | copy-start | bytes 1179652
  0.9 3.2 copy-start.8
  34.4 1.2 slice-start
  35.6 1.1 copy-start.6
  37.0 3.8 %slice-start.1 = ((bf16[16,304,128]{2,1,0:T(8,128)(2,1)}), bf16[16,192,128]{2,1,0:T(8,128)(2,1)S(1)}, s32[]{:S(2)}) async-start(bf16[16,304,128]{2,1,0:T(8,128)(2,1)} %shard_map.127), calls=%async_computation.1 | async-start | bytes 1572864 | tf_op jit(solution)/shard_map/slice | solution.py:358
  43.7 1.1 copy-start
  44.9 1.1 copy-start.1
  82.6 1.4 copy-start.5
  84.4 7.6 %copy-start.9 = (f32[2048]{0:T(1024)S(1)}, f32[2048]{0:T(1024)}, u32[]{:S(2)}) copy-start(f32[2048]{0:T(1024)} %param.20) | copy-start | bytes 24580
  88.5 3.5 %copy-start.2 = (bf16[192,2048]{1,0:T(8,128)(2,1)S(1)}, bf16[192,2048]{1,0:T(8,128)(2,1)}, u32[]{:S(2)}) copy-start(bf16[192,2048]{1,0:T(8,128)(2,1)} %convolution_convert_fusion.1) | copy-start | bytes 2359300
  88.5 3.5 %copy-start.4 = (bf16[96,2048]{1,0:T(8,128)(2,1)S(1)}, bf16[96,2048]{1,0:T(8,128)(2,1)}, u32[]{:S(2)}) copy-start(bf16[96,2048]{1,0:T(8,128)(2,1)} %param.13) | copy-start | bytes 1179652
  88.5 4.9 %copy-start.10 = (f32[2048]{0:T(1024)S(1)}, f32[2048]{0:T(1024)}, u32[]{:S(2)}) copy-start(f32[2048]{0:T(1024)} %param.21) | copy-start | bytes 24580
  90.6 2.8 copy-start.3
  240.5 7.2 %copy-start.12 = (bf16[16,128,352]{2,1,0:T(8,128)(2,1)S(1)}, bf16[16,128,352]{2,1,0:T(8,128)(2,1)}, u32[]{:S(2)}) copy-start(bf16[16,128,352]{2,1,0:T(8,128)(2,1)} %get-tuple-element.11) | copy-start | bytes 4325380
  322.8 2.7 copy-start.11

commit v2 on v1

--- a/solution.py
+++ b/solution.py
@@ -4,8 +4,10 @@
 import jax.numpy as jnp
 from jax import lax
 from jax.experimental import pallas as pl
+from jax.experimental.layout import Layout, with_layout_constraint
 from jax.experimental.pallas import tpu as pltpu
 from jax.sharding import PartitionSpec as P
+
 
 HD = 64
 
@@ -106,7 +108,7 @@
     carry, _ = lax.scan(
         advance, carry, (jnp.arange(blocks, dtype=jnp.int32), key_split, value_split)
     )
-    top, denom, accum = carry
+    _, denom, accum = carry
     attended = (accum / denom[..., None]).transpose(2, 0, 1, 3).reshape(rows, q_local * head_size)
     gated = (attended * jax.nn.sigmoid(out_gate.astype(jnp.float32))).astype(jnp.bfloat16)
     projected = lax.psum_scatter(
@@ -161,12 +163,19 @@
     )
 
 
+def mixed_order(size):
+    order = []
+    for j in range(1, size // 2 + 1):
+        order += [k for k in (size - 1 - j, j) if k and k not in order]
+    return order + [k for k in range(1, size) if k not in order]
+
+
 def swap_kernel(n, groups, x_ref, o_ref, send, recv, local):
     me = lax.axis_index("sp")
     size = n // groups
     slot = lax.rem(me, size)
     base = me - slot
-    peers = [base + lax.rem(slot + j, size) for j in range(1, size)]
+    peers = [base + (slot ^ j) for j in mixed_order(size)]
     greet([to(p) for p in peers])
     copies = []
     for j, p in enumerate(peers):
@@ -216,63 +225,94 @@
     )(x)
 
 
-def spread_kernel(n, groups, rows_ref, g_ref, u_ref, d_ref, all_ref, go_ref, uo_ref, do_ref,
-                  wsend, wrecv, wlocal, asend, arecv, psend, precv, alocal):
+def spread_kernel(n, groups, rows_ref, all_ref, asend, arecv, psend, precv, alocal):
     me = lax.axis_index("sp")
     core = lax.axis_index("tp")
     size = n // groups
     slot = lax.rem(me, size)
     base = me - slot
     mate = {"tp": 1 - core}
-    order = [lax.rem(me + j, n) for j in range(1, n)]
-    greet([mate] + [to(p) for p in order])
+    others = [slot ^ j for j in mixed_order(size)]
+    greet([mate] + [to(base + p) for p in others])
+    mine = all_ref.at[core, slot]
+    relays = [remote(rows_ref, mine, psend.at[0], precv.at[0], mate)]
+    relays[0].start()
     pushes = []
-    for j in range(1, size):
-        c = remote(rows_ref, all_ref.at[core, slot], asend.at[j - 1], arecv.at[j - 1],
-                   to(base + lax.rem(slot + j, size)))
+    for j, p in enumerate(others):
+        c = remote(rows_ref, mine, asend.at[j], arecv.at[j], to(base + p))
         c.start()
         pushes.append(c)
-    relays = [remote(rows_ref, all_ref.at[core, slot], psend.at[0], precv.at[0], mate)]
-    relays[0].start()
-    own = pltpu.make_async_copy(rows_ref, all_ref.at[core, slot], alocal)
+    own = pltpu.make_async_copy(rows_ref, mine, alocal)
     own.start()
-    weights = []
-    parts = ((g_ref, go_ref), (u_ref, uo_ref), (d_ref, do_ref))
-    for j, p in enumerate(order):
-        for k, (src, dst) in enumerate(parts):
-            c = remote(src.at[lax.rem(p, size)], dst.at[me], wsend.at[k, j], wrecv.at[k, j], to(p))
-            c.start()
-            weights.append(c)
-    locals_ = [pltpu.make_async_copy(src.at[slot], dst.at[me], wlocal.at[k])
-               for k, (src, dst) in enumerate(parts)]
-    for c in locals_:
-        c.start()
-    for j in range(1, size):
-        pushes[j - 1].wait()
-        origin = lax.rem(slot + size - j, size)
-        c = remote(all_ref.at[core, origin], all_ref.at[core, origin], psend.at[j], precv.at[j], mate)
+    for j, p in enumerate(others):
+        pushes[j].wait_recv()
+        c = remote(all_ref.at[core, p], all_ref.at[core, p], psend.at[j + 1], precv.at[j + 1], mate)
         c.start()
         relays.append(c)
     own.wait()
-    for c in relays + locals_ + weights:
+    for c in pushes:
+        c.wait_send()
+    for c in relays:
         c.wait()
 
 
-def spread(rows, g, u, d, n, groups, cid):
+def spread(rows, n, groups, cid):
     size = n // groups
-    full = lambda w: jax.ShapeDtypeStruct((n,) + w.shape[1:], w.dtype)
     dma = pltpu.SemaphoreType.DMA
     return pl.pallas_call(
         functools.partial(spread_kernel, n, groups),
-        out_shape=(jax.ShapeDtypeStruct((2, size) + rows.shape, rows.dtype), full(g), full(u), full(d)),
-        in_specs=[ANY] * 4,
-        out_specs=(ANY,) * 4,
-        scratch_shapes=[
-            dma((3, n - 1)), dma((3, n - 1)), dma((3,)),
-            dma((size - 1,)), dma((size - 1,)), dma((size,)), dma((size,)), dma,
-        ],
+        out_shape=jax.ShapeDtypeStruct((2, size) + rows.shape, rows.dtype),
+        in_specs=[ANY],
+        out_specs=ANY,
+        scratch_shapes=[dma((size - 1,)), dma((size - 1,)), dma((size,)), dma((size,)), dma],
         compiler_params=pltpu.CompilerParams(collective_id=cid, has_side_effects=True),
-    )(rows, g, u, d)
+    )(rows)
+
+
+def hidden_blocks(gate_weight, up_weight, down_weight, size):
+    ff = gate_weight.shape[1] // size
+    cut = lambda w: w.reshape(w.shape[0], size, ff).transpose(1, 0, 2)
+    blocks = jnp.stack([cut(gate_weight), cut(up_weight), cut(down_weight.T)], axis=1)
+    return with_layout_constraint(blocks, Layout(major_to_minor=(0, 1, 2, 3)))
+
+
+def ship(blocks, shifts, n, after):
+    me = lax.axis_index("sp")
+    blocks, after = lax.optimization_barrier((blocks, after))
+    arrived = {}
+    for j in shifts:
+        got = lax.dynamic_index_in_dim(blocks, lax.rem(me ^ j, blocks.shape[0]), 0, keepdims=False)
+        got = with_layout_constraint(got, Layout(major_to_minor=(0, 1, 2)))
+        arrived[j] = lax.ppermute(got, "sp", [(i, i ^ j) for i in range(n)])
+    return arrived, after
+
+
+def collect_kernel(shifts, *refs):
+    *arrived, out_ref, sems = refs
+    me = lax.axis_index("sp")
+    copies = []
+    for i, (j, src) in enumerate(zip(shifts, arrived)):
+        copies += [pltpu.make_async_copy(src.at[k], out_ref.at[k, me ^ j], sems.at[i, k])
+                   for k in range(src.shape[0])]
+    for c in copies:
+        c.start()
+    for c in copies:
+        c.wait()
+
+
+def collect(blocks, arrived, n):
+    me = lax.axis_index("sp")
+    own = lax.dynamic_index_in_dim(blocks, lax.rem(me, blocks.shape[0]), 0, keepdims=False)
+    arrived = {0: own, **arrived}
+    kinds = own.shape[0]
+    return pl.pallas_call(
+        functools.partial(collect_kernel, tuple(arrived)),
+        out_shape=jax.ShapeDtypeStruct((kinds, n) + own.shape[1:], own.dtype),
+        in_specs=[ANY] * len(arrived),
+        out_specs=pl.BlockSpec(memory_space=pltpu.VMEM),
+        scratch_shapes=[pltpu.SemaphoreType.DMA((len(arrived), kinds))],
+        compiler_params=pltpu.CompilerParams(vmem_limit_bytes=32 * 1024 * 1024),
+    )(*arrived.values())
 
 
 def attend_kernel(block, head, scale, q_ref, k_ref, v_ref, gc_ref, gr_ref, o_ref):
@@ -372,10 +412,14 @@
     groups = 2
     size = n // groups
     ff = gate_weight.shape[1] // size
+    blocks = hidden_blocks(gate_weight, up_weight, down_weight, size)
     got = swap(pack(queries, keys, values, log_gates, heads), n, 1, 1)
+    early = list(range(size, size + 3)) + list(range(1, size))
+    first, got = ship(blocks, early, n, got)
     q, k, v, gates = unpack(got, rows)
     att = attend(q, k, v, gates, n * rows // 6)
     back = swap(halves(att.reshape(n, rows, HD), LANES), n, 1, 2)
+    second, back = ship(blocks, range(size + 3, n), n, back)
     attended = unhalves(back, HD).transpose(1, 0, 2).reshape(rows, heads * HD).astype(jnp.float32)
     gated = (attended * jax.nn.sigmoid(out_gate.astype(jnp.float32))).astype(jnp.bfloat16)
     partial = jnp.dot(gated, out_weight, preferred_element_type=jnp.float32)
@@ -385,16 +429,15 @@
     projected = mine(partial) + partner(partial, 3).astype(jnp.float32)
     mixed = resid.astype(jnp.float32) + rms_scale(projected, post_gain)
     normed = rms_scale(mixed, pre_gain).astype(jnp.bfloat16)
-    cut = lambda w: w.reshape(w.shape[0], size, ff).transpose(1, 0, 2)
-    normed_all, gw, uw, dw = spread(
-        normed, cut(gate_weight), cut(up_weight), down_weight.reshape(size, ff, -1), n, groups, 4
-    )
+    normed_all = spread(normed, n, groups, 4)
+    first, second, normed_all = lax.optimization_barrier((first, second, normed_all))
+    weights = collect(blocks, {**first, **second}, n)
     x = normed_all.reshape(2 * size * normed.shape[0], width)
-    gate = jnp.dot(x, gw.reshape(width, ff), preferred_element_type=jnp.float32)
-    up = jnp.dot(x, uw.reshape(width, ff), preferred_element_type=jnp.float32)
+    gw, uw, dw = [weights[i].reshape(width, ff) for i in range(3)]
+    gate = jnp.dot(x, gw, preferred_element_type=jnp.float32)
+    up = jnp.dot(x, uw, preferred_element_type=jnp.float32)
     hidden = (jax.nn.silu(gate) * up).astype(jnp.bfloat16)
-    down = dw.transpose(1, 0, 2).reshape(ff, width)
-    part = jnp.dot(hidden, down, preferred_element_type=jnp.float32).astype(jnp.bfloat16)
+    part = jnp.einsum("tf,df->td", hidden, dw, preferred_element_type=jnp.float32).astype(jnp.bfloat16)
     part = part.reshape(2, size * normed.shape[0], width)
     both = mine(part) + partner(part, 5).astype(jnp.float32)
     both = both.astype(jnp.bfloat16).reshape(size, normed.shape[0], width)
@@ -407,7 +450,7 @@
 
     def body(*args):
         queries, gate_weight = args[1], args[10]
-        fits = cores == 2 and queries.shape[1] == n * HD and n % 2 == 0
+        fits = cores == 2 and queries.shape[1] == n * HD and n & (n - 1) == 0
         fits = fits and gate_weight.shape[1] % (n * 8) == 0
         return fast_shards(n, *args) if fits else shards(*args)
 

time: 333 us -> 339 us (1.018); the launches traced: 327 us -> 338 us
  Pallas kernels: 267 us -> 163 us
  starting transfers between devices: 0 us -> 70.5 us
  waiting for transfers between devices: 0 us -> 40 us
  local copies, waits for them, and re-layouts: 19.8 us -> 28.4 us
  matrix products: 23.1 us -> 19.4 us
    pallas_call x1 -> x2, Pallas kernels: 146 us -> 51.9 us  [the longest x1 45.9 us: spread(): pl.pallas_call(functools.partial(spread_kernel, n, groups), out_shape=jax...]
    ppermute x0 -> x15, starting transfers between devices: none -> 70.5 us  [ship(): arrived[j] = lax.ppermute(got, 'sp', [(i, i ^ j) for i in range(n)])]
    ppermute x0 -> x15, waiting for transfers between devices: none -> 40 us  [ship(): arrived[j] = lax.ppermute(got, 'sp', [(i, i ^ j) for i in range(n)])]
    pallas_call x3, Pallas kernels: 97.8 us -> 88.3 us  [swap(): pl.pallas_call(functools.partial(swap_kernel, n, groups), out_shape=jax.S...]
    squeeze x0 -> x3, local copies, waits for them, and re-layouts: none -> 6.67 us  [the longest x2 5.67 us: ship(): lax.dynamic_index_in_dim(blocks, lax.rem(me ^ j, blocks.shape[0]), 0, kee...]
    dot_general x2, matrix products: 19 us -> 15.3 us  [the longest x1 11.5 us: fast_shards(): jnp.einsum('tf,df->td', hidden, dw, preferred_element_type=jnp.float32)]
    unnamed x35 -> x41, local copies, waits for them, and re-layouts: 7.68 us -> 6.58 us
  transfers between devices with their start and end apart: 0 -> 15, of which waited for: 0 -> 6; matrix products, arithmetic and copies ran while one was open for 0% -> 4% of each run, Pallas kernels for 0% -> 14%
where the time goes in v2:
time: 339 us; the launch traced here: 338 us
  Pallas kernels  163 us (48%)
  starting transfers between devices  70.5 us (21%)
  waiting for transfers between devices  40 us (12%)
  local copies, waits for them, and re-layouts  28.4 us (8%)
  matrix products  19.4 us (6%)
  other arithmetic  16.2 us (5%)
    pallas_call x3, Pallas kernels, swap(): pl.pallas_call(functools.partial(swap_kernel, n, groups), out_shape=jax.S...  88.3 us
    ppermute x15, starting transfers between devices, ship(): arrived[j] = lax.ppermute(got, 'sp', [(i, i ^ j) for i in range(n)])  70.5 us
    pallas_call x1, Pallas kernels, spread(): pl.pallas_call(functools.partial(spread_kernel, n, groups), out_shape=jax...  45.9 us
    ppermute x15, waiting for transfers between devices, ship(): arrived[j] = lax.ppermute(got, 'sp', [(i, i ^ j) for i in range(n)])  40 us
    pallas_call x1, Pallas kernels, attend(): pl.pallas_call(functools.partial(attend_kernel, block, head, head ** (-0....  15.2 us
    dot_general x1, matrix products, fast_shards(): jnp.einsum('tf,df->td', hidden, dw, preferred_element_type=jnp.float32)  11.5 us
    pallas_call x2, Pallas kernels, partner(): pl.pallas_call(partner_kernel, out_shape=jax.ShapeDtypeStruct(x.shape[1:]...  8.1 us
  transfers between devices with their start and end apart: 15, of which 6 were waited for; matrix products, arithmetic and copies ran while one was open for 4% of the time, Pallas kernels for 14%

profile of v2, /device:TPU:0, one launch (start us, length us, event | category | flops | bytes accessed | tf_op | source)
XLA Modules:
  0.0 338.4 jit_solution(10877777520416487702)
XLA Ops:
  0.0 0.7 fusion.6
  0.9 1.0 copy.25
  2.1 1.0 copy.27
  3.3 1.2 copy.23
  4.5 0.4 copy.24
  5.2 1.5 pad_maximum_fusion.1.x_ref
  6.6 33.7 %shard_map.127 = bf16[16,304,128]{2,1,0:T(8,128)(2,1)} custom-call(bf16[16,304,128]{2,1,0:T(8,128)(2,1)} %pad_maximum_fusion.1.x_ref), custom_call_target="tpu_custom_call" | custom-call | tf_op jit(solution)/shard_map/pallas_call | solution.py:194
  40.4 0.3 copy.18
  40.7 0.4 copy.19
  41.1 0.3 copy.20
  41.5 0.4 copy.21
  41.8 1.5 copy.22
  43.3 1.9 pad_maximum_fusion
  45.3 0.8 slice-done
  46.4 1.4 add.174.gc_ref
  47.8 1.0 copy.31
  48.8 2.2 copy.32
  51.0 0.3 fusion.10
  51.3 0.8 copy-done.6
  52.3 15.2 %shard_map.128 = bf16[3072,64]{1,0:T(8,128)(2,1)S(1)} custom-call(bf16[3072,64]{1,0:T(8,128)(2,1)S(1)} %get-tuple-element.64.q_ref, bf16[3072,64]{1,0:T(8,128)(2,1)S(1)} %get-tuple-element.63.k_ref, bf16[3072,128]{1,0:T(8,128)(2,1)S(1)} %concatenate.11.v_ref, f32[3072,1]{1,0:T(8,128)S(1)} %add.174.gc_ref, f32[1,3072]{1,0:T(1,128)S(1)} %add.147.gr_ref), custom_call_target="tpu_custom_call" | custom-call | tf_op jit(solution)/shard_map/pallas_call | solution.py:347
  67.5 0.3 copy.34
  67.8 1.0 copy.35.x_ref
  68.8 15.1 %shard_map.129 = bf16[16,96,128]{2,1,0:T(8,128)(2,1)} custom-call(bf16[16,96,128]{2,1,0:T(8,128)(2,1)} %copy.35.x_ref), custom_call_target="tpu_custom_call" | custom-call | tf_op jit(solution)/shard_map/pallas_call | solution.py:194
  83.9 2.5 dynamic-slice_bitcast_fusion.1
  86.4 2.3 collective-permute-start.14
  88.7 2.7 collective-permute-start.13
  91.4 2.1 collective-permute-start.12
  93.5 2.3 collective-permute-start.11
  95.9 0.2 copy.38
  96.1 0.2 copy.36
  96.3 1.8 copy.37
  98.1 1.8 reshape.185
  100.0 0.3 fusion.2
  100.3 4.1 %convolution_convert_fusion.1 = bf16[192,2048]{1,0:T(8,128)(2,1)} fusion(bf16[192,1024]{0,1:T(8,128)(2,1)S(1)} %fusion.2, bf16[1024,2048]{1,0:T(8,128)(2,1)} %param.19), kind=kOutput, calls=%fused_computation.6 | convolution fusion | flops 805699584 | bytes 5373952 | tf_op jit(solution)/shard_map/dot_general | solution.py:425
  104.4 2.1 shard_map.130
  106.6 3.2 dynamic-slice_bitcast_fusion.6
  109.8 0.2 multiply_reduce_fusion.2
  110.0 21.0 %collective-permute-start.9 = (bf16[3,128,352]{2,1,0:T(8,128)(2,1)S(1)}, bf16[3,128,352]{2,1,0:T(8,128)(2,1)S(1)}, u32[]{:S(2)}, u32[]{:S(2)}) collective-permute-start(bf16[3,128,352]{2,1,0:T(8,128)(2,1)S(1)} %get-tuple-element.53), channel_id=1, source_target_pairs={{0,20},{2,22},{4,16},{6,18},{8,28},{10,30},{12,24},{14,26},{16,4},... | collective-permute-start | bytes 811016 | tf_op jit(solution)/shard_map/ppermute | solution.py:286
  131.0 11.3 %collective-permute-start.8 = (bf16[3,128,352]{2,1,0:T(8,128)(2,1)S(1)}, bf16[3,128,352]{2,1,0:T(8,128)(2,1)S(1)}, u32[]{:S(2)}, u32[]{:S(2)}) collective-permute-start(bf16[3,128,352]{2,1,0:T(8,128)(2,1)S(1)} %get-tuple-element.54), channel_id=1, source_target_pairs={{0,18},{2,16},{4,22},{6,20},{8,26},{10,24},{12,30},{14,28},{16,2},... | collective-permute-start | bytes 811016 | tf_op jit(solution)/shard_map/ppermute | solution.py:286
  142.3 12.6 %collective-permute-start.7 = (bf16[3,128,352]{2,1,0:T(8,128)(2,1)S(1)}, bf16[3,128,352]{2,1,0:T(8,128)(2,1)S(1)}, u32[]{:S(2)}, u32[]{:S(2)}) collective-permute-start(bf16[3,128,352]{2,1,0:T(8,128)(2,1)S(1)} %get-tuple-element.55), channel_id=1, source_target_pairs={{0,16},{2,18},{4,20},{6,22},{8,24},{10,26},{12,28},{14,30},{16,0},... | collective-permute-start | bytes 811016 | tf_op jit(solution)/shard_map/ppermute | solution.py:286
  154.9 12.9 %collective-permute-start.6 = (bf16[3,128,352]{2,1,0:T(8,128)(2,1)S(1)}, bf16[3,128,352]{2,1,0:T(8,128)(2,1)S(1)}, u32[]{:S(2)}, u32[]{:S(2)}) collective-permute-start(bf16[3,128,352]{2,1,0:T(8,128)(2,1)S(1)} %get-tuple-element.56), channel_id=1, source_target_pairs={{0,14},{2,12},{4,10},{6,8},{8,6},{10,4},{12,2},{14,0},{16,30},{18,... | collective-permute-start | bytes 811016 | tf_op jit(solution)/shard_map/ppermute | solution.py:286
  167.7 6.1 %collective-permute-done.10.refs_11_ = bf16[3,128,352]{2,1,0:T(8,128)(2,1)S(1)} collective-permute-done((bf16[3,128,352]{2,1,0:T(8,128)(2,1)}, bf16[3,128,352]{2,1,0:T(8,128)(2,1)S(1)}, u32[]{:S(2)}, u32[]{:S(2)}) %collective-permute-start.10) | collective-permute-done | bytes 270368 | tf_op jit(solution)/shard_map/ppermute | solution.py:286
  173.9 0.4 multiply_reduce_fusion.1
  174.2 6.6 %collective-permute-done.9.refs_10_ = bf16[3,128,352]{2,1,0:T(8,128)(2,1)S(1)} collective-permute-done((bf16[3,128,352]{2,1,0:T(8,128)(2,1)S(1)}, bf16[3,128,352]{2,1,0:T(8,128)(2,1)S(1)}, u32[]{:S(2)}, u32[]{:S(2)}) %collective-permute-start.9) | collective-permute-done | bytes 270368 | tf_op jit(solution)/shard_map/ppermute | solution.py:286
  180.8 6.8 %collective-permute-done.8.refs_9_ = bf16[3,128,352]{2,1,0:T(8,128)(2,1)S(1)} collective-permute-done((bf16[3,128,352]{2,1,0:T(8,128)(2,1)S(1)}, bf16[3,128,352]{2,1,0:T(8,128)(2,1)S(1)}, u32[]{:S(2)}, u32[]{:S(2)}) %collective-permute-start.8) | collective-permute-done | bytes 270368 | tf_op jit(solution)/shard_map/ppermute | solution.py:286
  187.6 5.1 %collective-permute-done.7.refs_8_ = bf16[3,128,352]{2,1,0:T(8,128)(2,1)S(1)} collective-permute-done((bf16[3,128,352]{2,1,0:T(8,128)(2,1)S(1)}, bf16[3,128,352]{2,1,0:T(8,128)(2,1)S(1)}, u32[]{:S(2)}, u32[]{:S(2)}) %collective-permute-start.7) | collective-permute-done | bytes 270368 | tf_op jit(solution)/shard_map/ppermute | solution.py:286
  192.7 1.0 collective-permute-start.2
  193.8 4.9 %collective-permute-done.6.refs_7_ = bf16[3,128,352]{2,1,0:T(8,128)(2,1)S(1)} collective-permute-done((bf16[3,128,352]{2,1,0:T(8,128)(2,1)S(1)}, bf16[3,128,352]{2,1,0:T(8,128)(2,1)S(1)}, u32[]{:S(2)}, u32[]{:S(2)}) %collective-permute-start.6) | collective-permute-done | bytes 270368 | tf_op jit(solution)/shard_map/ppermute | solution.py:286
  198.7 1.3 collective-permute-start.1
  200.0 10.4 %collective-permute-done.5.refs_6_ = bf16[3,128,352]{2,1,0:T(8,128)(2,1)S(1)} collective-permute-done((bf16[3,128,352]{2,1,0:T(8,128)(2,1)S(1)}, bf16[3,128,352]{2,1,0:T(8,128)(2,1)S(1)}, u32[]{:S(2)}, u32[]{:S(2)}) %collective-permute-start.5) | collective-permute-done | bytes 270368 | tf_op jit(solution)/shard_map/ppermute | solution.py:286
  210.5 1.0 collective-permute-start
  211.4 1.0 multiply_convert_fusion.rows_ref
  212.4 45.9 %shard_map.131 = bf16[2,8,96,2048]{3,2,1,0:T(8,128)(2,1)} custom-call(bf16[96,2048]{1,0:T(8,128)(2,1)} %multiply_convert_fusion.rows_ref), custom_call_target="tpu_custom_call" | custom-call | tf_op jit(solution)/shard_map/pallas_call | solution.py:262
  258.3 1.0 dynamic-slice_bitcast_fusion.refs_0_
  259.4 6.0 %shard_map.132 = bf16[3,16,128,352]{3,2,1,0:T(8,128)(2,1)S(1)} custom-call(bf16[3,128,352]{2,1,0:T(8,128)(2,1)S(1)} %dynamic-slice_bitcast_fusion.refs_0_, bf16[3,128,352]{2,1,0:T(8,128)(2,1)} %collective-permute-done.refs_1_, bf16[3,128,352]{2,1,0:T(8,128)(2,1)} %collective-permute-done.1.refs_2_, bf16[3,128,352]{2,1,0:T(8,128)(2,1)} %collective-permute-done.2.refs_3_, ...), custom_call_target="tpu_custom_call" | custom-call | tf_op jit(solution)/shard_map/pallas_call | solution.py:308
  265.4 0.6 fusion.9
  266.0 1.5 slice-done.4
  267.6 3.8 %fusion.11 = f32[1536,352]{0,1:T(8,128)} fusion(bf16[1536,2048]{1,0:T(8,128)(2,1)S(1)} %bitcast.148, bf16[2048,352]{1,0:T(8,128)(2,1)S(1)} %bitcast.163), kind=kOutput, calls=%fused_computation.55 | convolution fusion | flops 2214592512 | bytes 9895936 | tf_op jit(solution)/shard_map/dot_general | solution.py:437
  271.3 11.5 %convolution_convert_fusion = bf16[1536,2048]{1,0:T(8,128)(2,1)} fusion(bf16[2048,352]{1,0:T(8,128)(2,1)S(1)} %bitcast.161, bf16[1536,2048]{1,0:T(8,128)(2,1)} %bitcast.145, bf16[2048,352]{1,0:T(8,128)(2,1)S(1)} %bitcast.162, f32[1536,352]{0,1:T(8,128)} %fusion.11), kind=kOutput, calls=%fused_computation | convolution fusion | flops 4435574784 | bytes 17629184 | tf_op jit(solution)/shard_map/tf,df->td/dot_general | solution.py:440
  282.8 6.0 %shard_map.133 = bf16[768,2048]{1,0:T(8,128)(2,1)} custom-call(bf16[2,768,2048]{2,1,0:T(8,128)(2,1)} %bitcast.135), custom_call_target="tpu_custom_call" | custom-call | tf_op jit(solution)/shard_map/pallas_call | solution.py:218
  288.9 6.1 %fusion = bf16[768,2048]{1,0:T(8,128)(2,1)} fusion(bf16[768,2048]{1,0:T(8,128)(2,1)} %shard_map.133, bf16[2,768,2048]{2,1,0:T(8,128)(2,1)} %bitcast.136, s32[]{:T(128)S(6)} %select_n.55), kind=kLoop, calls=%fused_computation.2 | loop fusion | flops 6291456 | bytes 9437188 | tf_op jit(solution)/shard_map/convert_element_type | solution.py:443
  295.0 39.4 %shard_map.134 = bf16[8,96,2048]{2,1,0:T(8,128)(2,1)} custom-call(bf16[8,96,2048]{2,1,0:T(8,128)(2,1)} %bitcast.137), custom_call_target="tpu_custom_call" | custom-call | tf_op jit(solution)/shard_map/pallas_call | solution.py:194
  334.5 2.6 convert_reduce_fusion
  337.3 1.1 add_convert_fusion
  (70 shorter events, 1.5 us)
Async XLA Ops:
  5.1 35.2 %copy-start.8 = (bf16[128,2816]{1,0:T(8,128)(2,1)S(1)}, bf16[128,2816]{1,0:T(8,128)(2,1)}, u32[]{:S(2)}) copy-start(bf16[128,2816]{1,0:T(8,128)(2,1)} %param.23) | copy-start | bytes 2162692
  6.6 34.5 %copy-start.9 = (bf16[128,2816]{1,0:T(8,128)(2,1)S(1)}, bf16[128,2816]{1,0:T(8,128)(2,1)}, u32[]{:S(2)}) copy-start(bf16[128,2816]{1,0:T(8,128)(2,1)} %param.24) | copy-start | bytes 2162692
  45.3 0.8 slice-start
  45.3 2.5 slice-start.1
  45.3 5.8 %slice-start.2 = ((bf16[16,304,128]{2,1,0:T(8,128)(2,1)}), bf16[16,192,128]{2,1,0:T(8,128)(2,1)S(1)}, s32[]{:S(2)}) async-start(bf16[16,304,128]{2,1,0:T(8,128)(2,1)} %shard_map.127), calls=%async_computation.2 | async-start | bytes 1572864 | tf_op jit(solution)/shard_map/slice | solution.py:398
  51.0 1.1 copy-start.6
  67.8 28.1 %copy-start.10 = (bf16[192,1024]{1,0:T(8,128)(2,1)S(1)}, bf16[192,1024]{1,0:T(8,128)(2,1)}, u32[]{:S(2)}) copy-start(bf16[192,1024]{1,0:T(8,128)(2,1)} %param.18) | copy-start | bytes 1179652
  83.9 12.2 %copy-start.7 = (bf16[16,96,128]{2,1,0:T(8,128)(2,1)S(1)}, bf16[16,96,128]{2,1,0:T(8,128)(2,1)}, u32[]{:S(2)}) copy-start(bf16[16,96,128]{2,1,0:T(8,128)(2,1)} %shard_map.129) | copy-start | bytes 1179652
  86.4 23.6 %collective-permute-start.14 = (bf16[3,128,352]{2,1,0:T(8,128)(2,1)}, bf16[3,128,352]{2,1,0:T(8,128)(2,1)S(1)}, u32[]{:S(2)}, u32[]{:S(2)}) collective-permute-start(bf16[3,128,352]{2,1,0:T(8,128)(2,1)} %get-tuple-element.48), channel_id=1, source_target_pairs={{0,30},{2,28},{4,26},{6,24},{8,22},{10,20},{12,18},{14,16},{16,14}... | collective-permute-start | bytes 811016 | tf_op jit(solution)/shard_map/ppermute | solution.py:286
  88.7 42.2 %collective-permute-start.13 = (bf16[3,128,352]{2,1,0:T(8,128)(2,1)}, bf16[3,128,352]{2,1,0:T(8,128)(2,1)S(1)}, u32[]{:S(2)}, u32[]{:S(2)}) collective-permute-start(bf16[3,128,352]{2,1,0:T(8,128)(2,1)} %get-tuple-element.49), channel_id=1, source_target_pairs={{0,28},{2,30},{4,24},{6,26},{8,20},{10,22},{12,16},{14,18},{16,12}... | collective-permute-start | bytes 811016 | tf_op jit(solution)/shard_map/ppermute | solution.py:286
  91.4 50.9 %collective-permute-start.12 = (bf16[3,128,352]{2,1,0:T(8,128)(2,1)}, bf16[3,128,352]{2,1,0:T(8,128)(2,1)S(1)}, u32[]{:S(2)}, u32[]{:S(2)}) collective-permute-start(bf16[3,128,352]{2,1,0:T(8,128)(2,1)} %get-tuple-element.50), channel_id=1, source_target_pairs={{0,26},{2,24},{4,30},{6,28},{8,18},{10,16},{12,22},{14,20},{16,10}... | collective-permute-start | bytes 811016 | tf_op jit(solution)/shard_map/ppermute | solution.py:286
  93.5 61.3 %collective-permute-start.11 = (bf16[3,128,352]{2,1,0:T(8,128)(2,1)}, bf16[3,128,352]{2,1,0:T(8,128)(2,1)S(1)}, u32[]{:S(2)}, u32[]{:S(2)}) collective-permute-start(bf16[3,128,352]{2,1,0:T(8,128)(2,1)} %get-tuple-element.51), channel_id=1, source_target_pairs={{0,24},{2,26},{4,28},{6,30},{8,16},{10,18},{12,20},{14,22},{16,8},... | collective-permute-start | bytes 811016 | tf_op jit(solution)/shard_map/ppermute | solution.py:286
  95.9 78.0 %collective-permute-start.10 = (bf16[3,128,352]{2,1,0:T(8,128)(2,1)}, bf16[3,128,352]{2,1,0:T(8,128)(2,1)S(1)}, u32[]{:S(2)}, u32[]{:S(2)}) collective-permute-start(bf16[3,128,352]{2,1,0:T(8,128)(2,1)} %get-tuple-element.52), channel_id=1, source_target_pairs={{0,22},{2,20},{4,18},{6,16},{8,30},{10,28},{12,26},{14,24},{16,6},... | collective-permute-start | bytes 811016 | tf_op jit(solution)/shard_map/ppermute | solution.py:286
  106.5 3.2 copy-start
  106.5 3.2 copy-start.2
  106.5 67.3 %copy-start.4 = (bf16[96,2048]{1,0:T(8,128)(2,1)S(1)}, bf16[96,2048]{1,0:T(8,128)(2,1)}, u32[]{:S(2)}) copy-start(bf16[96,2048]{1,0:T(8,128)(2,1)} %param.13) | copy-start | bytes 1179652
  106.6 67.3 %copy-start.11 = (f32[2048]{0:T(1024)S(1)}, f32[2048]{0:T(1024)}, u32[]{:S(2)}) copy-start(f32[2048]{0:T(1024)} %param.20) | copy-start | bytes 24580
  106.6 104.8 %copy-start.12 = (f32[2048]{0:T(1024)S(1)}, f32[2048]{0:T(1024)}, u32[]{:S(2)}) copy-start(f32[2048]{0:T(1024)} %param.21) | copy-start | bytes 24580
  110.0 70.8 %collective-permute-start.9 = (bf16[3,128,352]{2,1,0:T(8,128)(2,1)S(1)}, bf16[3,128,352]{2,1,0:T(8,128)(2,1)S(1)}, u32[]{:S(2)}, u32[]{:S(2)}) collective-permute-start(bf16[3,128,352]{2,1,0:T(8,128)(2,1)S(1)} %get-tuple-element.53), channel_id=1, source_target_pairs={{0,20},{2,22},{4,16},{6,18},{8,28},{10,30},{12,24},{14,26},{16,4},... | collective-permute-start | bytes 811016 | tf_op jit(solution)/shard_map/ppermute | solution.py:286
  131.0 56.6 %collective-permute-start.8 = (bf16[3,128,352]{2,1,0:T(8,128)(2,1)S(1)}, bf16[3,128,352]{2,1,0:T(8,128)(2,1)S(1)}, u32[]{:S(2)}, u32[]{:S(2)}) collective-permute-start(bf16[3,128,352]{2,1,0:T(8,128)(2,1)S(1)} %get-tuple-element.54), channel_id=1, source_target_pairs={{0,18},{2,16},{4,22},{6,20},{8,26},{10,24},{12,30},{14,28},{16,2},... | collective-permute-start | bytes 811016 | tf_op jit(solution)/shard_map/ppermute | solution.py:286
  142.3 50.5 %collective-permute-start.7 = (bf16[3,128,352]{2,1,0:T(8,128)(2,1)S(1)}, bf16[3,128,352]{2,1,0:T(8,128)(2,1)S(1)}, u32[]{:S(2)}, u32[]{:S(2)}) collective-permute-start(bf16[3,128,352]{2,1,0:T(8,128)(2,1)S(1)} %get-tuple-element.55), channel_id=1, source_target_pairs={{0,16},{2,18},{4,20},{6,22},{8,24},{10,26},{12,28},{14,30},{16,0},... | collective-permute-start | bytes 811016 | tf_op jit(solution)/shard_map/ppermute | solution.py:286
  154.9 43.8 %collective-permute-start.6 = (bf16[3,128,352]{2,1,0:T(8,128)(2,1)S(1)}, bf16[3,128,352]{2,1,0:T(8,128)(2,1)S(1)}, u32[]{:S(2)}, u32[]{:S(2)}) collective-permute-start(bf16[3,128,352]{2,1,0:T(8,128)(2,1)S(1)} %get-tuple-element.56), channel_id=1, source_target_pairs={{0,14},{2,12},{4,10},{6,8},{8,6},{10,4},{12,2},{14,0},{16,30},{18,... | collective-permute-start | bytes 811016 | tf_op jit(solution)/shard_map/ppermute | solution.py:286
  173.9 36.6 %collective-permute-start.5 = (bf16[3,128,352]{2,1,0:T(8,128)(2,1)S(1)}, bf16[3,128,352]{2,1,0:T(8,128)(2,1)S(1)}, u32[]{:S(2)}, u32[]{:S(2)}) collective-permute-start(bf16[3,128,352]{2,1,0:T(8,128)(2,1)S(1)} %get-tuple-element.57), channel_id=1, source_target_pairs={{0,12},{2,14},{4,8},{6,10},{8,4},{10,6},{12,0},{14,2},{16,28},{18,... | collective-permute-start | bytes 811016 | tf_op jit(solution)/shard_map/ppermute | solution.py:286
  180.8 78.5 %collective-permute-start.4 = (bf16[3,128,352]{2,1,0:T(8,128)(2,1)}, bf16[3,128,352]{2,1,0:T(8,128)(2,1)S(1)}, u32[]{:S(2)}, u32[]{:S(2)}) collective-permute-start(bf16[3,128,352]{2,1,0:T(8,128)(2,1)} %get-tuple-element.58), channel_id=1, source_target_pairs={{0,10},{2,8},{4,14},{6,12},{8,2},{10,0},{12,6},{14,4},{16,26},{18,... | collective-permute-start | bytes 811016 | tf_op jit(solution)/shard_map/ppermute | solution.py:286
  187.6 71.7 %collective-permute-start.3 = (bf16[3,128,352]{2,1,0:T(8,128)(2,1)}, bf16[3,128,352]{2,1,0:T(8,128)(2,1)S(1)}, u32[]{:S(2)}, u32[]{:S(2)}) collective-permute-start(bf16[3,128,352]{2,1,0:T(8,128)(2,1)} %get-tuple-element.59), channel_id=1, source_target_pairs={{0,8},{2,10},{4,12},{6,14},{8,0},{10,2},{12,4},{14,6},{16,24},{18,... | collective-permute-start | bytes 811016 | tf_op jit(solution)/shard_map/ppermute | solution.py:286
  192.7 66.6 %collective-permute-start.2 = (bf16[3,128,352]{2,1,0:T(8,128)(2,1)}, bf16[3,128,352]{2,1,0:T(8,128)(2,1)}, u32[]{:S(2)}, u32[]{:S(2)}) collective-permute-start(bf16[3,128,352]{2,1,0:T(8,128)(2,1)} %get-tuple-element.60), channel_id=1, source_target_pairs={{0,6},{2,4},{4,2},{6,0},{8,14},{10,12},{12,10},{14,8},{16,22},{18,... | collective-permute-start | bytes 811016 | tf_op jit(solution)/shard_map/ppermute | solution.py:286
  198.7 60.7 %collective-permute-start.1 = (bf16[3,128,352]{2,1,0:T(8,128)(2,1)}, bf16[3,128,352]{2,1,0:T(8,128)(2,1)}, u32[]{:S(2)}, u32[]{:S(2)}) collective-permute-start(bf16[3,128,352]{2,1,0:T(8,128)(2,1)} %get-tuple-element.61), channel_id=1, source_target_pairs={{0,4},{2,6},{4,0},{6,2},{8,12},{10,14},{12,8},{14,10},{16,20},{18,... | collective-permute-start | bytes 811016 | tf_op jit(solution)/shard_map/ppermute | solution.py:286
  210.5 48.9 %collective-permute-start = (bf16[3,128,352]{2,1,0:T(8,128)(2,1)}, bf16[3,128,352]{2,1,0:T(8,128)(2,1)}, u32[]{:S(2)}, u32[]{:S(2)}) collective-permute-start(bf16[3,128,352]{2,1,0:T(8,128)(2,1)} %get-tuple-element.62), channel_id=1, source_target_pairs={{0,2},{2,0},{4,6},{6,4},{8,10},{10,8},{12,14},{14,12},{16,18},{18,... | collective-permute-start | bytes 811016 | tf_op jit(solution)/shard_map/ppermute | solution.py:286
  259.4 6.6 %slice-start.3 = ((s8[6291456]{0:T(1024)(128)(4,1)}), s8[2097152]{0:T(1024)(128)(4,1)S(1)}, s32[]{:S(2)}) async-start(s8[6291456]{0:T(1024)(128)(4,1)} %bitcast.146), calls=%async_computation.3 | async-start | bytes 4194304
  265.4 2.2 slice-start.4
  334.4 2.9 copy-start.1
  334.4 2.9 copy-start.3
  334.4 2.9 copy-start.5
  334.4 2.9 copy-start.13
